TPU v7x, 256 devices: a 2x2x32 block of a 4x8x32 slice. The times are simulated.
256 devices in a mesh: grp: 4 (over y, x), ep: 64 (over z, core).
Axes of the slice: x: 2, y: 2, z: 32, core: 2. Of those that a mesh axis runs over, the one named last changes fastest.
The devices are a block of a 4x8x32 slice.
Arguments:
- tokens: bfloat16 [2048, 2048], P(('grp', 'ep')), parts along dimension 0, may hold values from -6 to 6
- routes: int32 [2048, 4], P(('grp', 'ep')), parts along dimension 0, may hold values from 0 to 63, all different within a row; in each aligned block of 8 rows (0 to 7, 8 to 15, ...) at most 2 rows name the same one
- gate_weights: float32 [2048, 4], P(('grp', 'ep')), parts along dimension 0, may hold values from 0.1 to 1
- norm_gain: float32 [2048], replicated, may hold values from 0.1 to 1.9
- final_gain: float32 [2048], replicated, may hold values from 0.1 to 1.9
- w_gate: bfloat16 [64, 2048, 512], P('ep'), may hold values from -0.088388348 to 0.088388348
- w_up: bfloat16 [64, 2048, 512], P('ep'), may hold values from -0.088388348 to 0.088388348
- w_down: bfloat16 [64, 512, 2048], P('ep'), may hold values from -0.176776695 to 0.176776695
Outputs:
- mixed: bfloat16 [2048, 2048], P('grp', 'ep'), parts along dimension 0
There are 4 independent parts, one for each index of `grp`. A program takes and returns all parts, laid end to end along the dimension named above; an argument that names none is the same for every part. Nothing has to cross between parts.
Inputs may be any that keep to these rules, and one draw needn't show every extreme that they name: `routes`: each row names 4 different experts; among the rows of one device no expert is named by more than 2 rows, and some expert reaches 2.
All inputs are finite; a program needn't handle non-finite values.
Results may differ from a plain program's by a relative error of at most 0.008.
Values may be sent and summed in bfloat16 or wider, within the bound.
No kernel may reach another device: no remote copies, remote signals or barrier semaphores. Data moves between devices by JAX's collectives and lax.ppermute only.
A program may use at most 64 MiB of HBM per device.

v0:
```python
import jax
import jax.numpy as jnp
from jax import lax
from jax.sharding import Mesh
from jax.sharding import PartitionSpec as P

EP = ("ep_0", "ep_1")
GRP_EP = ("grp", "ep_0", "ep_1")


def in_blocks(shard, dim, peers):
    dims = shard.shape
    tiles = shard.reshape(*dims[:dim], peers, dims[dim] // peers, *dims[dim + 1 :])
    return jnp.moveaxis(tiles, dim, 0)


def in_order(tiles, dim):
    dims = list(tiles.shape[1:])
    dims[dim] *= tiles.shape[0]
    return jnp.moveaxis(tiles, 0, dim).reshape(dims)


def turned_blocks(tiles, axes, order):
    inside = tiles.shape[1:]
    whole = tiles.reshape(*(lax.axis_size(a) for a in axes), *inside)
    for k in order:
        whole = lax.all_to_all(whole, axes[k], k, k, tiled=True)
    return whole.reshape(-1, *inside)


def exchange_by_chip(shard, groups, order, split_dim, concat_dim):
    peers = lax.axis_size(groups[0]) * lax.axis_size(groups[1])
    tiles = in_blocks(shard, split_dim, peers)
    return in_order(turned_blocks(tiles, groups, order), concat_dim)


def expert_rows(rows, w_gate, w_up, w_down):
    gate_val = jnp.dot(rows, w_gate[0], preferred_element_type=jnp.float32)
    up_val = jnp.dot(rows, w_up[0], preferred_element_type=jnp.float32)
    act = (jax.nn.silu(gate_val) * up_val).astype(jnp.bfloat16)
    return jnp.dot(act, w_down[0], preferred_element_type=jnp.float32).astype(jnp.bfloat16)


def shards(tokens, routes, gate_weights, norm_gain, final_gain, w_gate, w_up, w_down):
    epsilon = 1e-06
    width = tokens.shape[1]
    topk = routes.shape[1]
    group = lax.axis_size(EP)
    per_dev = tokens.shape[0]
    most = max(2, (2 * per_dev * topk + group - 1) // group)
    values = tokens.astype(jnp.float32)
    normed = (
        values * lax.rsqrt(jnp.mean(values * values, axis=1, keepdims=True) + epsilon) * norm_gain
    ).astype(jnp.bfloat16)
    slots = jnp.arange(most, dtype=jnp.int32)
    experts = jnp.arange(group, dtype=jnp.int32)
    match = (routes[:, :, None] == experts[None, None, :]).astype(jnp.float32)
    row_used = jnp.sum(match, axis=1)
    row_gate = jnp.sum(match * gate_weights[:, :, None], axis=1)
    order_pos = jnp.cumsum(row_used, axis=0).astype(jnp.int32) - 1
    select = jnp.transpose(row_used)[:, None, :] * (
        jnp.transpose(order_pos)[:, None, :] == slots[None, :, None]
    ).astype(jnp.float32)
    outgoing = jnp.einsum(
        "ecr,rd->ecd", select.astype(jnp.bfloat16), normed, preferred_element_type=jnp.float32
    ).astype(jnp.bfloat16)
    received = lax.all_to_all(outgoing, EP, split_axis=0, concat_axis=0, tiled=True)
    count = received.shape[1]
    result = expert_rows(received.reshape(-1, width), w_gate, w_up, w_down)
    returned = lax.all_to_all(
        result.reshape(group, count, width), EP, split_axis=0, concat_axis=0, tiled=True
    )
    weights = select * jnp.transpose(row_gate)[:, None, :]
    combined = jnp.einsum(
        "ecr,ecd->rd", weights, returned.astype(jnp.float32), precision=lax.Precision.HIGHEST
    )
    scale = lax.rsqrt(jnp.mean(combined * combined, axis=1, keepdims=True) + epsilon)
    finished = (combined * scale * final_gain).astype(jnp.bfloat16)
    return exchange_by_chip(finished, ("ep_0", "ep_1"), (1, 0), 1, 0)


def solution(mesh):
    split = Mesh(mesh.devices.reshape(mesh.shape["grp"], 32, 2), ("grp", "ep_0", "ep_1"))
    return jax.shard_map(
        shards,
        mesh=split,
        in_specs=(
            P(GRP_EP, None),
            P(GRP_EP, None),
            P(GRP_EP, None),
            P(),
            P(),
            P(EP, None, None),
            P(EP, None, None),
            P(EP, None, None),
        ),
        out_specs=P("grp", EP),
        check_vma=False,
    )
```

profile of v0, /device:TPU:46, one launch (start us, length us, event | category | flops | bytes accessed | tf_op | source)
XLA Modules:
  0.0 209.5 jit_solution(14360317351344725999)
XLA Ops:
  0.0 0.0 copy-start
  0.0 1.0 fusion.20
  1.0 0.8 select_reduce_fusion
  1.9 1.1 convolution_convert_fusion.1
  3.0 0.5 copy.33
  3.5 98.2 %all_to_all.20 = bf16[64,2,2048]{2,1,0:T(2,128)(2,1)S(1)} all-to-all(bf16[64,2,2048]{2,1,0:T(2,128)(2,1)S(1)} %copy.33), channel_id=1, replica_groups=mesh['grp'=4,'ep_0'=32,'ep_1'=2] {'ep_0','ep_1'}, dimensions={0} | all-to-all | bytes 1048576 | tf_op jit(solution)/shard_map/all_to_all | solution.py:67
  101.8 0.2 reshape.35
  102.0 2.0 fusion.3
  104.0 0.0 copy-done
  104.0 2.4 %convolution_convert_fusion = bf16[128,2048]{1,0:T(8,128)(2,1)S(1)} fusion(bf16[1,512,2048]{2,1,0:T(8,128)(2,1)S(1)} %copy-done, bf16[128,2048]{1,0:T(8,128)(2,1)S(1)} %reshape.35, bf16[1,2048,512]{2,1,0:T(8,128)(2,1)} %param.14, f32[128,512]{1,0:T(8,128)S(1)} %fusion.3), kind=kOutput, calls=%fused_computation | convolution fusion | flops 537526272 | bytes 5505024 | tf_op jit(solution)/shard_map/dot_general | solution.py:41
  106.5 0.0 copy-start.1
  106.5 0.3 reshape.36
  106.8 69.9 %all_to_all.21 = bf16[64,2,2048]{2,1,0:T(2,128)(2,1)S(1)} all-to-all(bf16[64,2,2048]{2,1,0:T(2,128)(2,1)S(1)} %reshape.36), channel_id=1, replica_groups=mesh['grp'=4,'ep_0'=32,'ep_1'=2] {'ep_0','ep_1'}, dimensions={0} | all-to-all | bytes 1048576 | tf_op jit(solution)/shard_map/all_to_all | solution.py:70
  176.7 0.5 multiply_reduce_fusion
  177.3 0.0 copy-done.1
  177.3 0.1 multiply_convert_fusion
  177.4 0.2 reshape.37
  177.5 0.1 copy.43
  177.6 0.2 reshape.41
  177.8 3.8 %all_to_all.22 = bf16[2,2,4096]{2,1,0:T(2,128)(2,1)S(1)} all-to-all(bf16[2,2,4096]{2,1,0:T(2,128)(2,1)S(1)} %reshape.41), channel_id=1, replica_groups=mesh['grp'=4,'ep_0'=32,'ep_1'=2] {'ep_1'}, dimensions={0} | all-to-all | bytes 65536 | tf_op jit(solution)/shard_map/all_to_all | solution.py:27
  181.6 0.1 reshape.42
  181.7 0.1 reshape.43
  181.9 26.8 %all_to_all.23 = bf16[32,2,256]{2,1,0:T(2,128)(2,1)S(1)} all-to-all(bf16[32,2,256]{2,1,0:T(2,128)(2,1)S(1)} %reshape.43), channel_id=1, replica_groups=mesh['grp'=4,'ep_0'=32,'ep_1'=2] {'ep_0'}, dimensions={0} | all-to-all | bytes 65536 | tf_op jit(solution)/shard_map/all_to_all | solution.py:27
  208.7 0.1 reshape.44
  208.8 0.7 copy.37
  (5 shorter events, 0.1 us)
Async XLA Ops:
  0.0 104.0 %copy-start = (bf16[1,512,2048]{2,1,0:T(8,128)(2,1)S(1)}, bf16[1,512,2048]{2,1,0:T(8,128)(2,1)}, u32[]{:S(2)}) copy-start(bf16[1,512,2048]{2,1,0:T(8,128)(2,1)} %param.15) | copy-start | bytes 6291460
  106.5 70.8 %copy-start.1 = (f32[2048]{0:T(1024)S(1)}, f32[2048]{0:T(1024)}, u32[]{:S(2)}) copy-start(f32[2048]{0:T(1024)} %param.12) | copy-start | bytes 24580
where the time goes:
time: 210 us; the launch traced here: 209 us
  blocking collectives  199 us (95%)
  matrix products  6.1 us (3%)
  local copies, waits for them, and re-layouts  2.61 us (1%)
    all_to_all x1, blocking collectives, shards(): lax.all_to_all(outgoing, EP, split_axis=0, concat_axis=0, tiled=True)  98.2 us
    all_to_all x1, blocking collectives, shards(): lax.all_to_all(result.reshape(group, count, width), EP, split_axis=0, con...  69.9 us
    all_to_all x2, blocking collectives, turned_blocks(): whole = lax.all_to_all(whole, axes[k], k, k, tiled=True)  30.6 us

commit v1 on v0

v1 whole, which is shorter than its diff:
```python
import jax
import jax.numpy as jnp
from jax import lax
from jax.experimental import pallas as pl
from jax.experimental.pallas import tpu as pltpu
from jax.sharding import Mesh
from jax.sharding import PartitionSpec as P

EP = ("zh", "zl", "core")
GRP_EP = ("grp", "zh", "zl", "core")
LANES = 128


def swapped(parts, flag_low, flag_high):
    a, b, c, d = parts
    a, b, c, d = (
        jnp.where(flag_low, b, a),
        jnp.where(flag_low, a, b),
        jnp.where(flag_low, d, c),
        jnp.where(flag_low, c, d),
    )
    return (
        jnp.where(flag_high, c, a),
        jnp.where(flag_high, d, b),
        jnp.where(flag_high, a, c),
        jnp.where(flag_high, b, d),
    )


def combine_kernel(rows_ref, src_ref, lane_ref, out_ref):
    devices, cols, slots = rows_ref.shape
    tokens = src_ref.shape[1]
    topk = src_ref.shape[0]
    slot = lax.broadcasted_iota(jnp.int32, (slots, tokens), 0)
    src = src_ref[...]
    lane = lane_ref[...]

    def step(s, acc):
        key = jnp.where(src == s, lane, -1)
        hit = slot == key[0:1, :]
        for k in range(1, topk):
            hit = hit | (slot == key[k : k + 1, :])
        pick = jnp.where(hit, 1.0, 0.0).astype(jnp.bfloat16)
        return acc + jnp.dot(rows_ref[s], pick, preferred_element_type=jnp.float32)

    out_ref[...] = lax.fori_loop(
        0, devices, step, jnp.zeros((cols, tokens), jnp.float32), unroll=4
    )


def combine(rows, src, lane):
    return pl.pallas_call(
        combine_kernel,
        out_shape=jax.ShapeDtypeStruct((rows.shape[1], src.shape[1]), jnp.float32),
    )(rows, src, lane)


def shards(tokens, routes, gate_weights, norm_gain, final_gain, w_gate, w_up, w_down):
    epsilon = 1e-06
    per_dev, width = tokens.shape
    topk = routes.shape[1]
    group = lax.axis_size(EP)
    cols = width // group
    total = per_dev * group
    most = 2 * group
    me = lax.axis_index(EP)
    core = lax.axis_index("core")
    odd = lax.axis_index("zl")

    values = tokens.astype(jnp.float32)
    normed = (
        values * lax.rsqrt(jnp.mean(values * values, axis=1, keepdims=True) + epsilon) * norm_gain
    ).astype(jnp.bfloat16)
    high = lax.reduce_precision(gate_weights, 8, 7)
    rest = gate_weights - high
    mid = lax.reduce_precision(rest, 8, 7)
    low = rest - mid
    meta = jnp.concatenate([routes.astype(jnp.float32), high, mid, low], axis=1)
    used = meta.shape[1]
    meta = jnp.pad(meta, ((0, 0), (0, LANES - used))).astype(jnp.bfloat16)
    payload = jnp.concatenate([normed, meta], axis=1)

    chips = group // 2
    zigzag = []
    for chip in range(chips):
        zigzag.append((chip * 2, ((chip + 1) % chips) * 2))
        zigzag.append((chip * 2 + 1, ((chip - 1) % chips) * 2 + 1))
    swap = [(0, 1), (1, 0)]
    own = lax.all_gather(payload, "zh", axis=0, tiled=True)
    near = lax.ppermute(own, EP, zigzag)
    own_pair = lax.ppermute(own, "core", swap)
    near_pair = lax.ppermute(near, "core", swap)
    pieces = (own, own_pair, near, near_pair)
    part = own.shape[0]

    is_core = core == 1
    is_odd = odd == 1
    known = jnp.concatenate(
        [
            jnp.transpose(m)
            for m in swapped([p[:, width : width + topk] for p in pieces], is_core, is_odd)
        ],
        axis=1,
    ).astype(jnp.int32)

    experts = lax.broadcasted_iota(jnp.int32, (group, total), 0)
    hits = [(known[k : k + 1, :] == experts) for k in range(topk)]
    match = sum(h.astype(jnp.float32) for h in hits)
    before = (
        lax.broadcasted_iota(jnp.int32, (total, total), 0)
        < lax.broadcasted_iota(jnp.int32, (total, total), 1)
    ).astype(jnp.bfloat16)
    rank = jnp.dot(match.astype(jnp.bfloat16), before, preferred_element_type=jnp.float32)
    lane = jnp.stack([jnp.sum(jnp.where(h, rank, 0.0), axis=0) for h in hits]).astype(jnp.int32)
    mine = experts == me
    slot_of = jnp.sum(jnp.where(mine & (match > 0), rank + 1.0, 0.0), axis=0).astype(jnp.int32) - 1
    slot_of = jnp.concatenate(
        swapped([slot_of[k * part : (k + 1) * part] for k in range(4)], is_core, is_odd)
    )
    select = (
        lax.broadcasted_iota(jnp.int32, (most, total), 0) == slot_of[None, :]
    ).astype(jnp.bfloat16)
    rows = sum(
        jnp.dot(
            select[:, k * part : (k + 1) * part], pieces[k], preferred_element_type=jnp.float32
        )
        for k in range(4)
    )
    info = rows[:, width : width + used]
    gates = info[:, topk : 2 * topk] + info[:, 2 * topk : 3 * topk] + info[:, 3 * topk :]
    gate = jnp.sum(
        jnp.where(info[:, :topk] == me.astype(jnp.float32), gates, 0.0), axis=1, keepdims=True
    )
    rows = rows[:, :width].astype(jnp.bfloat16)

    gate_val = jnp.dot(rows, w_gate[0], preferred_element_type=jnp.float32)
    up_val = jnp.dot(rows, w_up[0], preferred_element_type=jnp.float32)
    act = (jax.nn.silu(gate_val) * up_val * gate).astype(jnp.bfloat16)
    result = lax.dot_general(
        w_down[0], act, (((0,), (1,)), ((), ())), preferred_element_type=jnp.float32
    ).astype(jnp.bfloat16)
    returned = lax.all_to_all(
        result.reshape(group, cols, most), EP, split_axis=0, concat_axis=0, tiled=True
    )
    mixed = combine(returned, known, lane)

    square = jnp.sum(mixed * mixed, axis=0)
    squares = lax.all_to_all(
        jnp.broadcast_to(square.astype(jnp.bfloat16)[None, :], (group, total)),
        EP,
        split_axis=0,
        concat_axis=0,
        tiled=True,
    )
    mean = jnp.sum(squares.astype(jnp.float32), axis=0, keepdims=True) / width
    gain = lax.dynamic_slice(final_gain, (me * cols,), (cols,))
    finished = (mixed * lax.rsqrt(mean + epsilon) * gain[:, None]).astype(jnp.bfloat16)
    finished = jnp.transpose(finished).reshape(4, part // per_dev, per_dev, cols)
    return jnp.swapaxes(finished, 0, 1).reshape(total, cols)


def solution(mesh):
    split = Mesh(mesh.devices.reshape(mesh.shape["grp"], 16, 2, 2), GRP_EP)
    return jax.shard_map(
        shards,
        mesh=split,
        in_specs=(
            P(GRP_EP, None),
            P(GRP_EP, None),
            P(GRP_EP, None),
            P(),
            P(),
            P(EP, None, None),
            P(EP, None, None),
            P(EP, None, None),
        ),
        out_specs=P("grp", EP),
        check_vma=False,
    )
```

time: 210 us -> 212 us (level)
  blocking collectives: 199 us -> 56.3 us
  waiting for transfers between devices: 0 us -> 98 us
  starting transfers between devices: 0 us -> 22.5 us
  Pallas kernels: 0 us -> 11.7 us
  local copies, waits for them, and re-layouts: 2.61 us -> 8.66 us
  other arithmetic: 1.95 us -> 6.24 us
    all_to_all x4 -> x0, blocking collectives: 199 us -> none  [the longest x1 98.2 us: shards(): lax.all_to_all(outgoing, EP, split_axis=0, concat_axis=0, tiled=True)]
    all_to_all x0 -> x2, waiting for transfers between devices: none -> 87.7 us  [the longest x1 63.6 us: shards(): lax.all_to_all(result.reshape(group, cols, most), EP, split_axis=0, conca...]
    all_gather x0 -> x1, blocking collectives: none -> 56.3 us  [shards(): own = lax.all_gather(payload, 'zh', axis=0, tiled=True)]
    all_to_all x0 -> x2, starting transfers between devices: none -> 19.8 us  [the longest x1 13.3 us: shards(): lax.all_to_all(result.reshape(group, cols, most), EP, split_axis=0, conca...]
    pallas_call x0 -> x1, Pallas kernels: none -> 11.7 us  [combine(): pl.pallas_call(combine_kernel, out_shape=jax.ShapeDtypeStruct((rows.shape...]
    ppermute x0 -> x3, waiting for transfers between devices: none -> 10.3 us  [the longest x1 8.26 us: shards(): near = lax.ppermute(own, EP, zigzag)]
    unnamed x8 -> x12, local copies, waits for them, and re-layouts: 0.56 us -> 3.38 us
    ppermute x0 -> x3, starting transfers between devices: none -> 2.69 us  [the longest x1 2.69 us: shards(): near = lax.ppermute(own, EP, zigzag)]
  transfers between devices with their start and end apart: 0 -> 5, of which waited for: 0 -> 4; matrix products, arithmetic and copies ran while one was open for 0% -> 1% of each run, Pallas kernels for 0% -> 0%
where the time goes in v1:
time: 212 us; the launch traced here: 211 us
  waiting for transfers between devices  98 us (46%)
  blocking collectives  56.3 us (27%)
  starting transfers between devices  22.5 us (11%)
  Pallas kernels  11.7 us (6%)
  local copies, waits for them, and re-layouts  8.66 us (4%)
  matrix products  7.5 us (4%)
  other arithmetic  6.24 us (3%)
    all_to_all x1, waiting for transfers between devices, shards(): lax.all_to_all(result.reshape(group, cols, most), EP, split_axis=0, conca...  63.6 us
    all_gather x1, blocking collectives, shards(): own = lax.all_gather(payload, 'zh', axis=0, tiled=True)  56.3 us
    all_to_all x1, waiting for transfers between devices, shards(): lax.all_to_all(jnp.broadcast_to(square.astype(jnp.bfloat16)[None, :], (gr...  24.1 us
    all_to_all x1, starting transfers between devices, shards(): lax.all_to_all(result.reshape(group, cols, most), EP, split_axis=0, conca...  13.3 us
    pallas_call x1, Pallas kernels, combine(): pl.pallas_call(combine_kernel, out_shape=jax.ShapeDtypeStruct((rows.shape...  11.7 us
    ppermute x1, waiting for transfers between devices, shards(): near = lax.ppermute(own, EP, zigzag)  8.26 us
    all_to_all x1, starting transfers between devices, shards(): lax.all_to_all(jnp.broadcast_to(square.astype(jnp.bfloat16)[None, :], (gr...  6.47 us
  transfers between devices with their start and end apart: 5, of which 4 were waited for; matrix products, arithmetic and copies ran while one was open for 1% of the time, Pallas kernels for 0%

profile of v1, /device:TPU:46, one launch (start us, length us, event | category | flops | bytes accessed | tf_op | source)
XLA Modules:
  0.0 211.1 jit_solution(17315195102011092151)
XLA Ops:
  0.0 0.0 copy-start
  0.0 0.9 copy.55
  0.9 0.8 copy.54
  1.7 0.9 fusion.29
  2.6 0.8 fusion.31
  3.4 0.1 fusion.51
  3.5 56.3 %all_gather.3 = bf16[128,2176]{1,0:T(8,128)(2,1)S(1)} all-gather(bf16[8,2176]{1,0:T(8,128)(2,1)S(1)} %pad_maximum_fusion), channel_id=1, replica_groups=mesh['grp'=4,'zh'=16,'zl'=2,'core'=2] {'zh'}, dimensions={0}, use_global_device_ids=true | all-gather | bytes 591872 | tf_op jit(solution)/shard_map/all_gather | solution.py:89
  59.8 1.0 copy.57
  60.9 2.7 %collective-permute-start = (bf16[128,2176]{0,1:T(8,128)(2,1)}, bf16[128,2176]{0,1:T(8,128)(2,1)S(1)}, u32[]{:S(2)}, u32[]{:S(2)}) collective-permute-start(bf16[128,2176]{0,1:T(8,128)(2,1)} %copy.57), channel_id=1, source_target_pairs={{0,2},{1,63},{2,4},{3,1},{4,6},{5,3},{6,8},{7,5},{8,10},{9,7},{10,... | collective-permute-start | bytes 1671176 | tf_op jit(solution)/shard_map/ppermute | solution.py:90
  63.6 0.0 collective-permute-start.2
  63.6 8.3 %collective-permute-done = bf16[128,2176]{0,1:T(8,128)(2,1)S(1)} collective-permute-done((bf16[128,2176]{0,1:T(8,128)(2,1)}, bf16[128,2176]{0,1:T(8,128)(2,1)S(1)}, u32[]{:S(2)}, u32[]{:S(2)}) %collective-permute-start) | collective-permute-done | bytes 557088 | tf_op jit(solution)/shard_map/ppermute | solution.py:90
  71.8 0.0 collective-permute-start.1
  71.8 0.0 collective-permute-done.2
  71.8 2.1 collective-permute-done.1
  73.9 0.7 select_bitcast_fusion.3
  74.6 0.0 copy-start.3
  74.6 0.3 select_reduce_fusion.3
  75.0 0.3 fusion.41
  75.4 0.0 copy-done.3
  75.4 1.4 convolution_add_fusion.2
  76.7 0.3 convolution_add_fusion.1
  77.1 0.0 copy-start.2
  77.1 1.5 convolution_add_fusion
  78.6 0.2 copy-done.2
  78.8 0.4 fusion.4
  79.3 0.2 fusion.33
  79.5 0.0 copy-done
  79.5 3.3 %fusion = bf16[2048,128]{0,1:T(8,128)(2,1)} fusion(bf16[1,512,2048]{2,1,0:T(8,128)(2,1)S(1)} %copy-done, bf16[1,2048,512]{2,1,0:T(8,128)(2,1)} %param.14, f32[128,512]{1,0:T(8,128)S(1)} %fusion.4, f32[128,2176]{1,0:T(8,128)S(1)} %convolution_add_fusion, f32[128]{0:T(128)S(1)} %fusion.33), kind=kOutput, calls=%fused_computation.4 | convolution fusion | flops 537591808 | bytes 5505536 | tf_op jit(solution)/shard_map/dot_general | solution.py:139
  82.7 2.0 copy.60
  84.8 13.3 %all-to-all-start = ((bf16[64,32,128]{2,1,0:T(8,128)(2,1)}), bf16[64,32,128]{2,1,0:T(8,128)(2,1)S(1)}, u32[]{:S(2)}, u32[]{:S(2)}) async-start(bf16[64,32,128]{2,1,0:T(8,128)(2,1)} %bitcast.12), calls=%async_computation | async-start | bytes 1048576 | tf_op jit(solution)/shard_map/all_to_all | solution.py:142
  98.1 0.6 maximum_convert_fusion.lane_ref
  98.7 63.6 %all-to-all-done.rows_ref = bf16[64,32,128]{2,1,0:T(8,128)(2,1)S(1)} async-done(((bf16[64,32,128]{2,1,0:T(8,128)(2,1)}), bf16[64,32,128]{2,1,0:T(8,128)(2,1)S(1)}, u32[]{:S(2)}, u32[]{:S(2)}) %all-to-all-start) | async-done | bytes 524320 | tf_op jit(solution)/shard_map/all_to_all | solution.py:142
  162.3 0.0 copy-start.1
  162.3 0.8 copy-done.1
  163.1 11.7 %shard_map.82 = f32[32,512]{1,0:T(8,128)} custom-call(bf16[64,32,128]{2,1,0:T(8,128)(2,1)} %copy-done.1, s32[4,512]{1,0:T(4,128)} %copy-done.3, s32[4,512]{1,0:T(4,128)} %maximum_convert_fusion.lane_ref), custom_call_target="tpu_custom_call" | custom-call | tf_op jit(solution)/shard_map/pallas_call | solution.py:52
  174.8 0.9 multiply_reduce_fusion
  175.6 0.1 broadcast_in_dim.13
  175.7 0.5 broadcast.62
  176.2 1.0 reduce.1
  177.2 0.6 reshape.42
  177.9 6.5 %all-to-all-start.1 = ((bf16[64,2,256]{2,1,0:T(2,128)(2,1)}), bf16[64,2,256]{2,1,0:T(2,128)(2,1)S(1)}, u32[]{:S(2)}, u32[]{:S(2)}) async-start(bf16[64,2,256]{2,1,0:T(2,128)(2,1)} %reshape.42), calls=%async_computation.1 | async-start | bytes 131072 | tf_op jit(solution)/shard_map/all_to_all | solution.py:148
  184.4 0.8 dynamic_slice.3
  185.1 24.1 %all-to-all-done.1 = bf16[64,2,256]{2,1,0:T(2,128)(2,1)S(1)} async-done(((bf16[64,2,256]{2,1,0:T(2,128)(2,1)}), bf16[64,2,256]{2,1,0:T(2,128)(2,1)S(1)}, u32[]{:S(2)}, u32[]{:S(2)}) %all-to-all-start.1) | async-done | bytes 65568 | tf_op jit(solution)/shard_map/all_to_all | solution.py:148
  209.2 0.1 reshape.43
  209.3 0.9 fusion.43
  210.2 0.1 copy.62
  210.3 0.7 copy.64
  (14 shorter events, 0.2 us)
Async XLA Ops:
  0.0 79.5 %copy-start = (bf16[1,512,2048]{2,1,0:T(8,128)(2,1)S(1)}, bf16[1,512,2048]{2,1,0:T(8,128)(2,1)}, u32[]{:S(2)}) copy-start(bf16[1,512,2048]{2,1,0:T(8,128)(2,1)} %param.15) | copy-start | bytes 6291460
  60.9 11.0 %collective-permute-start = (bf16[128,2176]{0,1:T(8,128)(2,1)}, bf16[128,2176]{0,1:T(8,128)(2,1)S(1)}, u32[]{:S(2)}, u32[]{:S(2)}) collective-permute-start(bf16[128,2176]{0,1:T(8,128)(2,1)} %copy.57), channel_id=1, source_target_pairs={{0,2},{1,63},{2,4},{3,1},{4,6},{5,3},{6,8},{7,5},{8,10},{9,7},{10,... | collective-permute-start | bytes 1671176 | tf_op jit(solution)/shard_map/ppermute | solution.py:90
  63.6 8.3 %collective-permute-start.2 = (bf16[128,2176]{0,1:T(8,128)(2,1)}, bf16[128,2176]{0,1:T(8,128)(2,1)}, u32[]{:S(2)}, u32[]{:S(2)}) collective-permute-start(bf16[128,2176]{0,1:T(8,128)(2,1)} %copy.57), channel_id=1, source_target_pairs={{0,1},{1,0},{2,3},{3,2},{4,5},{5,4},{6,7},{7,6},{8,9},{9,8},{10,11... | collective-permute-start | bytes 1671176 | tf_op jit(solution)/shard_map/ppermute | solution.py:91
  71.8 2.1 collective-permute-start.1
  74.6 0.7 copy-start.3
  77.1 1.8 copy-start.2
  84.8 77.5 %all-to-all-start = ((bf16[64,32,128]{2,1,0:T(8,128)(2,1)}), bf16[64,32,128]{2,1,0:T(8,128)(2,1)S(1)}, u32[]{:S(2)}, u32[]{:S(2)}) async-start(bf16[64,32,128]{2,1,0:T(8,128)(2,1)} %bitcast.12), calls=%async_computation | async-start | bytes 1048576 | tf_op jit(solution)/shard_map/all_to_all | solution.py:142
  162.3 0.8 copy-start.1
  177.9 31.3 %all-to-all-start.1 = ((bf16[64,2,256]{2,1,0:T(2,128)(2,1)}), bf16[64,2,256]{2,1,0:T(2,128)(2,1)S(1)}, u32[]{:S(2)}, u32[]{:S(2)}) async-start(bf16[64,2,256]{2,1,0:T(2,128)(2,1)} %reshape.42), calls=%async_computation.1 | async-start | bytes 131072 | tf_op jit(solution)/shard_map/all_to_all | solution.py:148
